TPU v7x, 512 devices: a whole 4x4x16 slice. The times are simulated.
512 devices in a mesh: sp: 32 (over z, core), tp: 16 (over y, x).
Axes of the slice: x: 4, y: 4, z: 16, core: 2. Of those that a mesh axis runs over, the one named last changes fastest.
Arguments:
- residual: bfloat16 [8192, 2048], P('sp'), may hold values from -6 to 6
- queries: bfloat16 [8192, 16, 128], P('sp', 'tp'), may hold values from -256 to 256
- key_vectors: bfloat16 [8192, 16, 128], P('sp', 'tp'), may hold values from -5.3 to 5.3
- value_rows: bfloat16 [8192, 16, 128], P('sp', 'tp'), may hold values from -6 to 6
- head_lambda: float32 [16], P('tp'), may hold values from 0.3 to 0.8
- head_gain: float32 [128], replicated, may hold values from 0.1 to 1.9
- out_weight: bfloat16 [2048, 2048], P('tp'), may hold values from -0.125 to 0.125
- ffn_gain: float32 [2048], replicated, may hold values from 0.1 to 1.9
- expert_gate: bfloat16 [32, 2048, 4096], P('sp', None, 'tp'), may hold values from -0.125 to 0.125
- expert_up: bfloat16 [32, 2048, 4096], P('sp', None, 'tp'), may hold values from -0.125 to 0.125
- expert_down: bfloat16 [32, 4096, 2048], P('sp', None, 'tp'), may hold values from -0.09375 to 0.09375
- routing: int32 [8192, 2], P('sp'), may hold values from 0 to 31, as said below
- route_weight: float32 [8192, 2], P('sp'), may hold values from 0.1 to 0.9
Outputs:
- layer_out: bfloat16 [8192, 2048], P('sp')
Inputs may be any that keep to these rules, and one draw needn't show every extreme that they name: `routing`: each row names two different experts of one group of 8 consecutive experts. In each aligned block of 256 rows no expert is named by more than 32 rows, and in every block some expert is named by exactly 32 rows.
All inputs are finite; a program needn't handle non-finite values.
Results may differ from a plain program's by a relative error of at most 0.015.
Values may be sent and summed in bfloat16 or wider, within the bound.
No kernel may reach another device: no remote copies, remote signals or barrier semaphores. Data moves between devices by JAX's collectives and lax.ppermute only.
A program may use at most 64 MiB of HBM per device.

v0:
```python
import math
import jax
import jax.numpy as jnp
from jax import lax
from jax.sharding import PartitionSpec as P

GROUPS = 4
norm_eps = 1e-06


def sent_together(arrays, axis, dim, along):
    ends, at = ([], 0)
    for a in arrays[:-1]:
        at += a.shape[along]
        ends.append(at)
    both = jnp.concatenate(arrays, axis=along)
    return tuple(jnp.split(lax.all_gather(both, axis, axis=dim, tiled=True), ends, axis=along))


def in_blocks(array, dim, peers):
    before, after = (array.shape[:dim], array.shape[dim + 1 :])
    return jnp.moveaxis(array.reshape(*before, peers, -1, *after), dim, 0)


def sum_at_owner(array, axis, dim):
    parts = in_blocks(array, dim, lax.axis_size(axis))
    arrived = lax.all_to_all(parts, axis, split_axis=0, concat_axis=0, tiled=True)
    return arrived.astype(jnp.float32).sum(axis=0)


def padded_to(lines, peers):
    spare = -len(lines) % peers
    return jnp.pad(lines, [(0, spare)] + [(0, 0)] * (lines.ndim - 1))


def from_everyone(array, axis):
    peers = lax.axis_size(axis)
    return lax.all_to_all(
        jnp.broadcast_to(array[None], (peers, *array.shape)), axis, 0, 0, tiled=True
    )


def laid_out(parts, dim):
    parts = jnp.moveaxis(parts, 0, dim)
    dims = parts.shape
    return parts.reshape(*dims[:dim], dims[dim] * dims[dim + 1], *dims[dim + 2 :])


def collect(array, axis, dim):
    parts = from_everyone(array, axis)
    return laid_out(parts, dim)


def sum_by_parts(array, axes):
    lines = array.reshape(-1, array.shape[-1])
    own = sum_at_owner(padded_to(lines, lax.axis_size(axes)), axes, 0)
    whole = collect(own.astype(jnp.bfloat16), axes, 0)
    return whole[: len(lines)].reshape(array.shape).astype(jnp.float32)


def online_update(running, query_part, key_part, value_part, query_pos, key_pos, score_scale):
    highest, totals, accum = running
    scores = (
        jnp.einsum("qhd,khd->hqk", query_part, key_part, preferred_element_type=jnp.float32)
        * score_scale
    )
    scores = jnp.where(key_pos[None, None, :] <= query_pos[None, :, None], scores, -jnp.inf)
    new_high = jnp.maximum(highest, jnp.max(scores, axis=-1))
    shrink = jnp.exp(highest - new_high)
    weights = jnp.exp(scores - new_high[:, :, None])
    totals = shrink * totals + jnp.sum(weights, axis=-1)
    blended = jnp.einsum(
        "hqk,khe->qhe", weights.astype(jnp.bfloat16), value_part, preferred_element_type=jnp.float32
    )
    accum = jnp.transpose(shrink)[:, :, None] * accum + blended
    return (new_high, totals, accum)


def shards(
    residual,
    queries,
    key_vectors,
    value_rows,
    head_lambda,
    head_gain,
    out_weight,
    ffn_gain,
    expert_gate,
    expert_up,
    expert_down,
    routing,
    route_weight,
):
    tok_count = queries.shape[0]
    local_heads = queries.shape[1]
    half_width = queries.shape[2] // 2
    value_width = value_rows.shape[2]
    score_scale = half_width ** (-0.5)
    query_pos = lax.axis_index("sp") * tok_count + jnp.arange(tok_count, dtype=jnp.int32)
    last_query = query_pos[-1]
    first_half = queries[:, :, :half_width]
    second_half = queries[:, :, half_width:]
    start_high = jnp.full((local_heads, tok_count), -1e30, jnp.float32)
    start_total = jnp.zeros((local_heads, tok_count), jnp.float32)
    start_accum = jnp.zeros((tok_count, local_heads, value_width), jnp.float32)
    empty_state = (start_high, start_total, start_accum)
    running = (empty_state, empty_state)
    key_piece, value_piece = sent_together((key_vectors, value_rows), "sp", 0, 1)
    piece_len = key_piece.shape[0]
    block_len = math.gcd(piece_len, 512)
    block_count = piece_len // block_len
    key_blocks = key_piece.reshape(block_count, block_len, local_heads, 2 * half_width)
    value_blocks = value_piece.reshape(block_count, block_len, local_heads, value_width)

    def visit(current, stacked):
        block_index, key_block, value_block = stacked
        block_first = block_index * block_len
        key_pos = block_first + jnp.arange(block_len, dtype=jnp.int32)

        def compute(inside):
            first_state = online_update(
                inside[0],
                first_half,
                key_block[:, :, :half_width],
                value_block,
                query_pos,
                key_pos,
                score_scale,
            )
            second_state = online_update(
                inside[1],
                second_half,
                key_block[:, :, half_width:],
                value_block,
                query_pos,
                key_pos,
                score_scale,
            )
            return (first_state, second_state)

        return (lax.cond(block_first <= last_query, compute, lambda inside: inside, current), None)

    running, _ = lax.scan(
        visit, running, (jnp.arange(block_count, dtype=jnp.int32), key_blocks, value_blocks)
    )
    first_state, second_state = running
    first_out = first_state[2] / jnp.transpose(first_state[1])[:, :, None]
    second_out = second_state[2] / jnp.transpose(second_state[1])[:, :, None]
    combined = first_out - head_lambda[None, :, None] * second_out
    normed_heads = (
        combined
        * lax.rsqrt(jnp.mean(combined * combined, axis=-1, keepdims=True) + norm_eps)
        * head_gain
    )
    attended = normed_heads.astype(jnp.bfloat16).reshape(tok_count, local_heads * value_width)
    partial_proj = jnp.dot(attended, out_weight, preferred_element_type=jnp.float32)
    projected = sum_by_parts(partial_proj.astype(jnp.bfloat16), "tp")
    stream = residual.astype(jnp.float32) + projected
    block_normed = (
        stream * lax.rsqrt(jnp.mean(stream * stream, axis=-1, keepdims=True) + norm_eps) * ffn_gain
    ).astype(jnp.bfloat16)
    expert_count = lax.axis_size("sp")
    tp_count = lax.axis_size("tp")
    per_group = expert_count // GROUPS
    capacity = tok_count // per_group
    top_count = routing.shape[1]
    model_width = block_normed.shape[1]
    flat_routes = routing.reshape(-1)
    route_count = flat_routes.shape[0]
    onehot = (flat_routes[:, None] == jnp.arange(expert_count, dtype=jnp.int32)[None, :]).astype(
        jnp.int32
    )
    earlier = jnp.cumsum(onehot, axis=0) - onehot
    position = jnp.sum(earlier * onehot, axis=1)
    slot_index = flat_routes * capacity + position
    slot_token = (
        jnp.full((expert_count * capacity,), tok_count, jnp.int32)
        .at[slot_index]
        .set(jnp.arange(route_count, dtype=jnp.int32) // top_count)
    )
    slot_table = slot_token.reshape(expert_count, capacity)
    slice_width = model_width // tp_count
    own_columns = lax.dynamic_slice_in_dim(
        block_normed, lax.axis_index("tp") * slice_width, slice_width, 1
    )
    outgoing = jnp.take(own_columns, slot_table, axis=0, mode="fill", fill_value=0)
    landed = lax.all_to_all(outgoing, "sp", split_axis=0, concat_axis=0, tiled=True)
    arrived = collect(landed, "tp", 2)
    expert_rows = arrived.reshape(-1, model_width)
    gate_part = jnp.dot(expert_rows, expert_gate[0], preferred_element_type=jnp.float32)
    up_part = jnp.dot(expert_rows, expert_up[0], preferred_element_type=jnp.float32)
    inner_act = (jax.nn.silu(gate_part) * up_part).astype(jnp.bfloat16)
    down_width = expert_down.shape[2]
    weight_rows = expert_down[0]
    expert_sum = jnp.dot(
        lax.all_gather(inner_act, "tp", axis=1, tiled=True),
        weight_rows,
        preferred_element_type=jnp.float32,
    )
    expert_out = expert_sum.astype(jnp.bfloat16).reshape(expert_count, capacity, down_width)
    returned = lax.all_to_all(expert_out, "sp", split_axis=0, concat_axis=0, tiled=True)
    per_route = returned.reshape(expert_count * capacity, down_width)[slot_index]
    weighted = per_route.astype(jnp.float32) * route_weight.reshape(-1)[:, None]
    token_sum = jnp.sum(weighted.reshape(tok_count, top_count, down_width), axis=1)
    moe_rows = collect(token_sum.astype(jnp.bfloat16), "tp", 1).astype(token_sum.dtype)
    return (stream + moe_rows).astype(jnp.bfloat16)


def solution(mesh):
    in_specs = (
        P("sp", None),
        P("sp", "tp", None),
        P("sp", "tp", None),
        P("sp", "tp", None),
        P("tp"),
        P(),
        P("tp", None),
        P(),
        P("sp", None, "tp"),
        P("sp", None, "tp"),
        P("sp", None, "tp"),
        P("sp", None),
        P("sp", None),
    )
    out_specs = P("sp", None)
    return jax.shard_map(shards, mesh=mesh, in_specs=in_specs, out_specs=out_specs, check_vma=False)
```

profile of v0, /device:TPU:1, one launch (start us, length us, event | category | flops | bytes accessed | tf_op | source)
XLA Modules:
  0.0 460.8 jit_solution(17257785034887943455)
XLA Ops:
  6.5 1.6 pad_maximum_fusion
  8.2 0.6 slice.25
  8.9 1.0 fusion.59
  10.7 78.0 %all-gather.3.cloned.1.call-done = bf16[8192,2,128]{2,0,1:T(8,128)(2,1)} async-done(((bf16[256,2,128]{2,0,1:T(8,128)(2,1)}), bf16[8192,2,128]{2,0,1:T(8,128)(2,1)}) %all-gather.3.cloned.1.call-update) | async-done | bytes 4194320 | tf_op jit(solution)/shard_map/all_gather | solution.py:17
  88.7 3.8 fusion.58
  92.6 33.3 %while.21 = (s32[]{:T(128)}, f32[1,256]{1,0:T(1,128)S(1)}, f32[1,256]{1,0:T(1,128)S(1)}, f32[256,1,128]{0,2,1:T(8,128)S(1)}, f32[1,256]{1,0:T(1,128)S(1)}, /*ind...) while((s32[]{:T(128)}, f32[1,256]{1,0:T(1,128)S(1)}, ...), condition=%wide.region_7.8_spmd.clone, body=%wide.region_0.7_spmd.clone.sunk | while | flops 102893312 | bytes 4570543 | solution.py:143
  92.6 0.6 dynamic_slice.42
  94.5 2.4 conditional.3
  94.5 0.9 dynamic-slice_bitcast_fusion
  97.0 0.6 dynamic_slice.42
  98.9 0.6 dynamic_slice.42
  100.8 0.6 dynamic_slice.42
  102.8 0.6 dynamic_slice.42
  104.7 0.6 dynamic_slice.42
  106.6 0.6 dynamic_slice.42
  108.6 0.6 dynamic_slice.42
  110.5 0.6 dynamic_slice.42
  112.4 0.6 dynamic_slice.42
  114.4 0.6 dynamic_slice.42
  116.3 0.6 dynamic_slice.42
  118.2 0.6 dynamic_slice.42
  120.2 0.6 dynamic_slice.42
  122.1 0.6 dynamic_slice.42
  126.0 2.5 convolution_convert_fusion
  128.6 6.5 %all-to-all-start = ((bf16[16,16,2048]{2,1,0:T(8,128)(2,1)}), bf16[16,16,2048]{2,1,0:T(8,128)(2,1)S(1)}, u32[]{:S(2)}, u32[]{:S(2)}) async-start(bf16[16,16,2048]{2,1,0:T(8,128)(2,1)} %bitcast.29), calls=%async_computation | async-start | bytes 2097152 | tf_op jit(solution)/shard_map/all_to_all | solution.py:27
  135.6 1.2 reduce-window.6
  137.4 14.1 %all-to-all-done = bf16[16,16,2048]{2,1,0:T(8,128)(2,1)S(1)} async-done(((bf16[16,16,2048]{2,1,0:T(8,128)(2,1)}), bf16[16,16,2048]{2,1,0:T(8,128)(2,1)S(1)}, u32[]{:S(2)}, u32[]{:S(2)}) %all-to-all-start) | async-done | bytes 1048608 | tf_op jit(solution)/shard_map/all_to_all | solution.py:27
  151.7 1.1 broadcast_in_dim.38
  152.8 4.5 all-to-all-start.1
  157.4 2.4 scatter_custom_fusion
  160.0 0.8 dynamic-slice
  160.8 12.4 %all-to-all-done.1 = bf16[16,16,2048]{2,1,0:T(8,128)(2,1)S(1)} async-done(((bf16[16,16,2048]{2,1,0:T(8,128)(2,1)}), bf16[16,16,2048]{2,1,0:T(8,128)(2,1)S(1)}, u32[]{:S(2)}, u32[]{:S(2)}) %all-to-all-start.1) | async-done | bytes 1048608 | tf_op jit(solution)/shard_map/all_to_all | solution.py:38
  173.7 3.2 gather_fusion
  177.2 65.0 %all_to_all.30 = bf16[32,32,128]{2,1,0:T(8,128)(2,1)S(1)} all-to-all(bf16[32,32,128]{2,1,0:T(8,128)(2,1)S(1)} %broadcast_select_fusion), channel_id=1, replica_groups=mesh['sp'=32,'tp'=16] {'sp'}, dimensions={0} | all-to-all | bytes 524288 | tf_op jit(solution)/shard_map/all_to_all | solution.py:187
  242.1 0.8 broadcast_in_dim.42
  242.9 52.7 %all_to_all.31 = bf16[16,32,32,128]{3,2,1,0:T(8,128)(2,1)S(1)} all-to-all(bf16[16,32,32,128]{3,2,1,0:T(8,128)(2,1)S(1)} %broadcast_in_dim.42), channel_id=1, replica_groups=mesh['sp'=32,'tp'=16] {'tp'}, dimensions={0} | all-to-all | bytes 8388608 | tf_op jit(solution)/shard_map/all_to_all | solution.py:38
  295.6 4.9 %copy.34 = bf16[32,32,16,128]{3,2,1,0:T(8,128)(2,1)S(1)} copy(bf16[32,32,16,128]{3,1,0,2:T(8,128)(2,1)S(1)} %bitcast.139) | data formatting | bytes 8388608 | tf_op jit(solution)/shard_map/transpose | solution.py:44
  300.5 1.3 fusion.26
  301.8 2.1 fusion.34
  303.9 81.9 %all-gather.5.cloned.1.call-done = bf16[1024,4096]{1,0:T(8,128)(2,1)} async-done(((bf16[1024,256]{1,0:T(8,128)(2,1)}), bf16[1024,4096]{1,0:T(8,128)(2,1)}) %all-gather.5.cloned.1.call-update) | async-done | bytes 8388624 | tf_op jit(solution)/shard_map/all_gather | solution.py:196
  385.8 6.6 %convolution_convert_fusion.1 = bf16[1024,128]{1,0:T(8,128)(2,1)} fusion(bf16[1024,4096]{1,0:T(8,128)(2,1)} %all-gather.5.cloned.1.call-done, bf16[1,4096,128]{2,1,0:T(8,128)(2,1)} %param.27), kind=kOutput, calls=%fused_computation.53 | convolution fusion | flops 1073872896 | bytes 9699328 | tf_op jit(solution)/shard_map/dot_general | solution.py:195
  392.4 14.4 %all-to-all-start.4 = ((bf16[32,32,128]{2,1,0:T(8,128)(2,1)}), bf16[32,32,128]{2,1,0:T(8,128)(2,1)S(1)}, u32[]{:S(2)}, u32[]{:S(2)}) async-start(bf16[32,32,128]{2,1,0:T(8,128)(2,1)} %bitcast.151), calls=%async_computation.4 | async-start | bytes 524288 | tf_op jit(solution)/shard_map/all_to_all | solution.py:201
  406.8 0.8 copy.35
  407.6 21.5 %all-to-all-done.4 = bf16[32,32,128]{2,1,0:T(8,128)(2,1)S(1)} async-done(((bf16[32,32,128]{2,1,0:T(8,128)(2,1)}), bf16[32,32,128]{2,1,0:T(8,128)(2,1)S(1)}, u32[]{:S(2)}, u32[]{:S(2)}) %all-to-all-start.4) | async-done | bytes 262176 | tf_op jit(solution)/shard_map/all_to_all | solution.py:201
  429.1 1.3 gather_fusion.1
  430.4 1.3 fusion.40
  432.0 20.5 %all_to_all.32 = bf16[16,256,128]{2,1,0:T(8,128)(2,1)S(1)} all-to-all(bf16[16,256,128]{2,1,0:T(8,128)(2,1)S(1)} %broadcast_in_dim.43), channel_id=1, replica_groups=mesh['sp'=32,'tp'=16] {'tp'}, dimensions={0} | all-to-all | bytes 2097152 | tf_op jit(solution)/shard_map/all_to_all | solution.py:38
  452.5 1.5 fusion.30
  (115 shorter events, 5.1 us)
Async XLA Ops:
  6.5 294.0 %copy-start = (bf16[1,2048,256]{2,1,0:T(8,128)(2,1)S(1)}, bf16[1,2048,256]{2,1,0:T(8,128)(2,1)}, u32[]{:S(2)}) copy-start(bf16[1,2048,256]{2,1,0:T(8,128)(2,1)} %param.25) | copy-start | bytes 3145732
  6.5 82.2 %all-gather.3.cloned.1.call-start = ((), (), s32[]{:S(2)}) async-start(), calls=%async_computation.6 | async-start | bytes 4325376 | tf_op jit(solution)/shard_map/all_gather | solution.py:17
  92.6 33.4 %copy-start.4 = (f32[128]{0:T(128)S(1)}, f32[128]{0:T(128)}, u32[]{:S(2)}) copy-start(f32[128]{0:T(128)} %param.22) | copy-start | bytes 1540
  126.0 9.2 %copy-start.2 = (s32[256,2]{0,1:T(2,128)S(1)}, s32[256,2]{0,1:T(2,128)}, u32[]{:S(2)}) copy-start(s32[256,2]{0,1:T(2,128)} %param.28) | copy-start | bytes 6148
  128.6 23.0 %all-to-all-start = ((bf16[16,16,2048]{2,1,0:T(8,128)(2,1)}), bf16[16,16,2048]{2,1,0:T(8,128)(2,1)S(1)}, u32[]{:S(2)}, u32[]{:S(2)}) async-start(bf16[16,16,2048]{2,1,0:T(8,128)(2,1)} %bitcast.29), calls=%async_computation | async-start | bytes 2097152 | tf_op jit(solution)/shard_map/all_to_all | solution.py:27
  137.4 35.8 %copy-start.1 = (bf16[256,2048]{1,0:T(8,128)(2,1)S(1)}, bf16[256,2048]{1,0:T(8,128)(2,1)}, u32[]{:S(2)}) copy-start(bf16[256,2048]{1,0:T(8,128)(2,1)} %param.17) | copy-start | bytes 3145732
  152.8 20.4 %all-to-all-start.1 = ((bf16[16,16,2048]{2,1,0:T(8,128)(2,1)}), bf16[16,16,2048]{2,1,0:T(8,128)(2,1)S(1)}, u32[]{:S(2)}, u32[]{:S(2)}) async-start(bf16[16,16,2048]{2,1,0:T(8,128)(2,1)} %broadcast_in_dim.38), calls=%async_computation.1 | async-start | bytes 2097152 | tf_op jit(solution)/shard_map/all_to_all | solution.py:38
  157.3 228.5 %all-gather.5.cloned.1.call-start = ((), (), s32[]{:S(2)}) async-start(), calls=%async_computation.7 | async-start | bytes 8912896 | tf_op jit(solution)/shard_map/all_gather | solution.py:196
  300.5 1.3 copy-start.5
  303.9 102.9 %copy-start.3 = (f32[256,2]{0,1:T(2,128)S(1)}, f32[256,2]{0,1:T(2,128)}, u32[]{:S(2)}) copy-start(f32[256,2]{0,1:T(2,128)} %param.29) | copy-start | bytes 6148
  392.4 36.6 %all-to-all-start.4 = ((bf16[32,32,128]{2,1,0:T(8,128)(2,1)}), bf16[32,32,128]{2,1,0:T(8,128)(2,1)S(1)}, u32[]{:S(2)}, u32[]{:S(2)}) async-start(bf16[32,32,128]{2,1,0:T(8,128)(2,1)} %bitcast.151), calls=%async_computation.4 | async-start | bytes 524288 | tf_op jit(solution)/shard_map/all_to_all | solution.py:201
Sparse Core Ops, SparseCore 0:
  9.5 79.1 all-gather.2
  304.0 81.7 all-gather.4
where the time goes:
time: 462 us; the launch traced here: 461 us
  waiting for transfers between devices  208 us (45%)
  blocking collectives  138 us (30%)
  local copies, waits for them, and re-layouts  32.7 us (7%)
  starting transfers between devices  25.4 us (5%)
  loops' own time  21.5 us (5%)
  between operations  14.4 us (3%)
  matrix products  13.6 us (3%)
  other arithmetic  7.04 us (2%)
    all_gather x1, waiting for transfers between devices, shards(): lax.all_gather(inner_act, 'tp', axis=1, tiled=True)  81.9 us
    all_gather x1, waiting for transfers between devices, sent_together(): lax.all_gather(both, axis, axis=dim, tiled=True)  78 us
    all_to_all x2, blocking collectives, from_everyone(): lax.all_to_all(jnp.broadcast_to(array[None], (peers, *array.shape)), axis...  73.2 us
    all_to_all x1, blocking collectives, shards(): lax.all_to_all(outgoing, 'sp', split_axis=0, concat_axis=0, tiled=True)  65 us
    all_to_all x1, waiting for transfers between devices, shards(): lax.all_to_all(expert_out, 'sp', split_axis=0, concat_axis=0, tiled=True)  21.5 us
    another operation x1, loops' own time, shards(): lax.scan(visit, running, (jnp.arange(block_count, dtype=jnp.int32), key_b...  21.2 us
    all_to_all x1, starting transfers between devices, shards(): lax.all_to_all(expert_out, 'sp', split_axis=0, concat_axis=0, tiled=True)  14.4 us
    all_to_all x1, waiting for transfers between devices, sum_at_owner(): lax.all_to_all(parts, axis, split_axis=0, concat_axis=0, tiled=True)  14.1 us
  transfers between devices with their start and end apart: 5, of which 5 were waited for; matrix products, arithmetic and copies ran while one was open for 2% of the time, Pallas kernels for 0%

commit v1 on v0

--- a/solution.py
+++ b/solution.py
@@ -1,11 +1,26 @@
+import functools
 import math
 import jax
 import jax.numpy as jnp
 from jax import lax
 from jax.sharding import PartitionSpec as P
+from jax.lax import all_to_all, axis_size
 
 GROUPS = 4
 norm_eps = 1e-06
+
+
+def types_handle(message, array_dim):
+    nodes = axis_size("tp")
+    moved = range(message.ndim)
+    value_now = map(lambda dd: nodes if dd == array_dim else 1, moved)
+    long_array = list(value_now)
+    g_now = jnp.tile(message, long_array)
+    answer = all_to_all(g_now, "tp", split_axis=array_dim, concat_axis=array_dim, tiled=True)
+    return answer
+
+
+_number_waves = functools.partial(types_handle, array_dim=1)
 
 
 def sent_together(arrays, axis, dim, along):
@@ -192,11 +207,7 @@
     inner_act = (jax.nn.silu(gate_part) * up_part).astype(jnp.bfloat16)
     down_width = expert_down.shape[2]
     weight_rows = expert_down[0]
-    expert_sum = jnp.dot(
-        lax.all_gather(inner_act, "tp", axis=1, tiled=True),
-        weight_rows,
-        preferred_element_type=jnp.float32,
-    )
+    expert_sum = jnp.dot(_number_waves(inner_act), weight_rows, preferred_element_type=jnp.float32)
     expert_out = expert_sum.astype(jnp.bfloat16).reshape(expert_count, capacity, down_width)
     returned = lax.all_to_all(expert_out, "sp", split_axis=0, concat_axis=0, tiled=True)
     per_route = returned.reshape(expert_count * capacity, down_width)[slot_index]

time: 462 us -> 482 us (1.043)
  blocking collectives: 138 us -> 235 us
  waiting for transfers between devices: 208 us -> 126 us
  local copies, waits for them, and re-layouts: 32.7 us -> 45.8 us
  starting transfers between devices: 25.4 us -> 17.7 us
    all_to_all x0 -> x1, blocking collectives: none -> 98.3 us  [types_handle(): all_to_all(g_now, 'tp', split_axis=array_dim, concat_axis=array_dim, tile...]
    all_gather x1 -> x0, waiting for transfers between devices: 81.9 us -> none  [shards(): lax.all_gather(inner_act, 'tp', axis=1, tiled=True)]
    all_to_all x0 -> x1, local copies, waits for them, and re-layouts: none -> 12.3 us  [types_handle(): all_to_all(g_now, 'tp', split_axis=array_dim, concat_axis=array_dim, tile...]
    all_to_all x1, starting transfers between devices: 14.4 us -> 6.73 us  [shards(): lax.all_to_all(expert_out, 'sp', split_axis=0, concat_axis=0, tiled=True)]
  transfers between devices with their start and end apart: 5 -> 4, of which waited for: 5 -> 4; matrix products, arithmetic and copies ran while one was open for 2% -> 2% of each run, Pallas kernels for 0% -> 0%
where the time goes in v1:
time: 482 us; the launch traced here: 480 us
  blocking collectives  235 us (49%)
  waiting for transfers between devices  126 us (26%)
  local copies, waits for them, and re-layouts  45.8 us (10%)
  loops' own time  21.5 us (4%)
  starting transfers between devices  17.7 us (4%)
  between operations  14.4 us (3%)
  matrix products  12.9 us (3%)
  other arithmetic  7.04 us (1%)
    all_to_all x1, blocking collectives, types_handle(): all_to_all(g_now, 'tp', split_axis=array_dim, concat_axis=array_dim, tile...  98.3 us
    all_gather x1, waiting for transfers between devices, sent_together(): lax.all_gather(both, axis, axis=dim, tiled=True)  78 us
    all_to_all x2, blocking collectives, from_everyone(): lax.all_to_all(jnp.broadcast_to(array[None], (peers, *array.shape)), axis...  71.4 us
    all_to_all x1, blocking collectives, shards(): lax.all_to_all(outgoing, 'sp', split_axis=0, concat_axis=0, tiled=True)  64.9 us
    all_to_all x1, waiting for transfers between devices, shards(): lax.all_to_all(expert_out, 'sp', split_axis=0, concat_axis=0, tiled=True)  21.5 us
    another operation x1, loops' own time, shards(): lax.scan(visit, running, (jnp.arange(block_count, dtype=jnp.int32), key_b...  21.2 us
    all_to_all x1, waiting for transfers between devices, sum_at_owner(): lax.all_to_all(parts, axis, split_axis=0, concat_axis=0, tiled=True)  14.1 us
    all_to_all x1, waiting for transfers between devices, from_everyone(): lax.all_to_all(jnp.broadcast_to(array[None], (peers, *array.shape)), axis...  12.4 us
  transfers between devices with their start and end apart: 4, of which 4 were waited for; matrix products, arithmetic and copies ran while one was open for 2% of the time, Pallas kernels for 0%

profile of v1, /device:TPU:1, one launch (start us, length us, event | category | flops | bytes accessed | tf_op | source)
XLA Modules:
  0.0 480.1 jit_solution(16894597995826434151)
XLA Ops:
  6.5 1.6 pad_maximum_fusion
  8.2 0.6 slice.25
  8.9 1.0 fusion.59
  10.7 78.0 %all-gather.2.cloned.1.call-done = bf16[8192,2,128]{2,0,1:T(8,128)(2,1)} async-done(((bf16[256,2,128]{2,0,1:T(8,128)(2,1)}), bf16[8192,2,128]{2,0,1:T(8,128)(2,1)}) %all-gather.2.cloned.1.call-update) | async-done | bytes 4194320 | tf_op jit(solution)/shard_map/all_gather | solution.py:32
  88.7 3.8 fusion.58
  92.6 33.3 %while.21 = (s32[]{:T(128)}, f32[1,256]{1,0:T(1,128)S(1)}, f32[1,256]{1,0:T(1,128)S(1)}, f32[256,1,128]{0,2,1:T(8,128)S(1)}, f32[1,256]{1,0:T(1,128)S(1)}, /*ind...) while((s32[]{:T(128)}, f32[1,256]{1,0:T(1,128)S(1)}, ...), condition=%wide.region_7.8_spmd.clone, body=%wide.region_0.7_spmd.clone.sunk | while | flops 102893312 | bytes 4570543 | solution.py:158
  92.6 0.6 dynamic_slice.42
  94.5 2.4 conditional.3
  94.5 0.9 dynamic-slice_bitcast_fusion
  97.0 0.6 dynamic_slice.42
  98.9 0.6 dynamic_slice.42
  100.8 0.6 dynamic_slice.42
  102.8 0.6 dynamic_slice.42
  104.7 0.6 dynamic_slice.42
  106.6 0.6 dynamic_slice.42
  108.6 0.6 dynamic_slice.42
  110.5 0.6 dynamic_slice.42
  112.4 0.6 dynamic_slice.42
  114.4 0.6 dynamic_slice.42
  116.3 0.6 dynamic_slice.42
  118.2 0.6 dynamic_slice.42
  126.1 2.5 convolution_convert_fusion
  128.6 6.5 %all-to-all-start = ((bf16[16,16,2048]{2,1,0:T(8,128)(2,1)}), bf16[16,16,2048]{2,1,0:T(8,128)(2,1)S(1)}, u32[]{:S(2)}, u32[]{:S(2)}) async-start(bf16[16,16,2048]{2,1,0:T(8,128)(2,1)} %bitcast.29), calls=%async_computation | async-start | bytes 2097152 | tf_op jit(solution)/shard_map/all_to_all | solution.py:42
  135.6 1.2 reduce-window.6
  137.4 14.1 %all-to-all-done = bf16[16,16,2048]{2,1,0:T(8,128)(2,1)S(1)} async-done(((bf16[16,16,2048]{2,1,0:T(8,128)(2,1)}), bf16[16,16,2048]{2,1,0:T(8,128)(2,1)S(1)}, u32[]{:S(2)}, u32[]{:S(2)}) %all-to-all-start) | async-done | bytes 1048608 | tf_op jit(solution)/shard_map/all_to_all | solution.py:42
  151.7 1.1 broadcast_in_dim.38
  152.8 4.5 all-to-all-start.1
  157.3 2.4 scatter_custom_fusion
  160.0 0.8 dynamic-slice
  160.8 12.4 %all-to-all-done.1 = bf16[16,16,2048]{2,1,0:T(8,128)(2,1)S(1)} async-done(((bf16[16,16,2048]{2,1,0:T(8,128)(2,1)}), bf16[16,16,2048]{2,1,0:T(8,128)(2,1)S(1)}, u32[]{:S(2)}, u32[]{:S(2)}) %all-to-all-start.1) | async-done | bytes 1048608 | tf_op jit(solution)/shard_map/all_to_all | solution.py:53
  173.7 3.2 gather_fusion
  177.2 64.9 %all_to_all.39 = bf16[32,32,128]{2,1,0:T(8,128)(2,1)S(1)} all-to-all(bf16[32,32,128]{2,1,0:T(8,128)(2,1)S(1)} %broadcast_select_fusion), channel_id=1, replica_groups=mesh['sp'=32,'tp'=16] {'sp'}, dimensions={0} | all-to-all | bytes 524288 | tf_op jit(solution)/shard_map/all_to_all | solution.py:202
  242.1 0.8 broadcast_in_dim.42
  242.9 52.7 %all_to_all.40 = bf16[16,32,32,128]{3,2,1,0:T(8,128)(2,1)S(1)} all-to-all(bf16[16,32,32,128]{3,2,1,0:T(8,128)(2,1)S(1)} %broadcast_in_dim.42), channel_id=1, replica_groups=mesh['sp'=32,'tp'=16] {'tp'}, dimensions={0} | all-to-all | bytes 8388608 | tf_op jit(solution)/shard_map/all_to_all | solution.py:53
  295.6 4.9 %copy.45 = bf16[32,32,16,128]{3,2,1,0:T(8,128)(2,1)S(1)} copy(bf16[32,32,16,128]{3,1,0,2:T(8,128)(2,1)S(1)} %bitcast.140) | data formatting | bytes 8388608 | tf_op jit(solution)/shard_map/transpose | solution.py:59
  300.5 1.3 fusion.26
  301.8 1.3 fusion.34
  303.1 0.8 tile.2
  303.9 98.3 %all_to_all.41 = bf16[1024,16,256]{2,0,1:T(8,128)(2,1)} all-to-all(bf16[1024,16,256]{2,0,1:T(8,128)(2,1)S(1)} %tile.2), channel_id=1, replica_groups=mesh['sp'=32,'tp'=16] {'tp'}, dimensions={1} | all-to-all | bytes 16777216 | tf_op jit(solution)/shard_map/all_to_all | solution.py:19
  402.2 12.3 %copy.46 = bf16[1024,16,256]{0,2,1:T(8,128)(2,1)} copy(bf16[1024,16,256]{2,0,1:T(8,128)(2,1)} %all_to_all.41) | data formatting | bytes 16777216 | tf_op jit(solution)/shard_map/all_to_all | solution.py:19
  414.5 6.7 %convolution_convert_fusion.1 = bf16[1024,128]{1,0:T(8,128)(2,1)} fusion(bf16[1024,4096]{0,1:T(8,128)(2,1)} %bitcast.141, bf16[1,4096,128]{2,1,0:T(8,128)(2,1)} %param.27), kind=kOutput, calls=%fused_computation.53 | convolution fusion | flops 1073872896 | bytes 9699328 | tf_op jit(solution)/shard_map/dot_general | solution.py:210
  421.2 6.7 %all-to-all-start.5 = ((bf16[32,32,128]{2,1,0:T(8,128)(2,1)}), bf16[32,32,128]{2,1,0:T(8,128)(2,1)S(1)}, u32[]{:S(2)}, u32[]{:S(2)}) async-start(bf16[32,32,128]{2,1,0:T(8,128)(2,1)} %bitcast.153), calls=%async_computation.5 | async-start | bytes 524288 | tf_op jit(solution)/shard_map/all_to_all | solution.py:212
  428.0 0.8 copy.47
  428.7 21.5 %all-to-all-done.5 = bf16[32,32,128]{2,1,0:T(8,128)(2,1)S(1)} async-done(((bf16[32,32,128]{2,1,0:T(8,128)(2,1)}), bf16[32,32,128]{2,1,0:T(8,128)(2,1)S(1)}, u32[]{:S(2)}, u32[]{:S(2)}) %all-to-all-start.5) | async-done | bytes 262176 | tf_op jit(solution)/shard_map/all_to_all | solution.py:212
  450.2 1.3 gather_fusion.1
  451.5 1.3 fusion.40
  453.1 18.7 %all_to_all.42 = bf16[16,256,128]{2,1,0:T(8,128)(2,1)S(1)} all-to-all(bf16[16,256,128]{2,1,0:T(8,128)(2,1)S(1)} %broadcast_in_dim.43), channel_id=1, replica_groups=mesh['sp'=32,'tp'=16] {'tp'}, dimensions={0} | all-to-all | bytes 2097152 | tf_op jit(solution)/shard_map/all_to_all | solution.py:53
  471.8 1.5 fusion.30
  (115 shorter events, 6.2 us)
Async XLA Ops:
  6.5 293.9 %copy-start = (bf16[1,2048,256]{2,1,0:T(8,128)(2,1)S(1)}, bf16[1,2048,256]{2,1,0:T(8,128)(2,1)}, u32[]{:S(2)}) copy-start(bf16[1,2048,256]{2,1,0:T(8,128)(2,1)} %param.25) | copy-start | bytes 3145732
  6.5 82.2 %all-gather.2.cloned.1.call-start = ((), (), s32[]{:S(2)}) async-start(), calls=%async_computation.7 | async-start | bytes 4325376 | tf_op jit(solution)/shard_map/all_gather | solution.py:32
  92.6 33.4 %copy-start.4 = (f32[128]{0:T(128)S(1)}, f32[128]{0:T(128)}, u32[]{:S(2)}) copy-start(f32[128]{0:T(128)} %param.22) | copy-start | bytes 1540
  126.0 9.2 %copy-start.2 = (s32[256,2]{0,1:T(2,128)S(1)}, s32[256,2]{0,1:T(2,128)}, u32[]{:S(2)}) copy-start(s32[256,2]{0,1:T(2,128)} %param.28) | copy-start | bytes 6148
  128.6 23.0 %all-to-all-start = ((bf16[16,16,2048]{2,1,0:T(8,128)(2,1)}), bf16[16,16,2048]{2,1,0:T(8,128)(2,1)S(1)}, u32[]{:S(2)}, u32[]{:S(2)}) async-start(bf16[16,16,2048]{2,1,0:T(8,128)(2,1)} %bitcast.29), calls=%async_computation | async-start | bytes 2097152 | tf_op jit(solution)/shard_map/all_to_all | solution.py:42
  137.4 35.8 %copy-start.1 = (bf16[256,2048]{1,0:T(8,128)(2,1)S(1)}, bf16[256,2048]{1,0:T(8,128)(2,1)}, u32[]{:S(2)}) copy-start(bf16[256,2048]{1,0:T(8,128)(2,1)} %param.17) | copy-start | bytes 3145732
  152.8 20.4 %all-to-all-start.1 = ((bf16[16,16,2048]{2,1,0:T(8,128)(2,1)}), bf16[16,16,2048]{2,1,0:T(8,128)(2,1)S(1)}, u32[]{:S(2)}, u32[]{:S(2)}) async-start(bf16[16,16,2048]{2,1,0:T(8,128)(2,1)} %broadcast_in_dim.38), calls=%async_computation.1 | async-start | bytes 2097152 | tf_op jit(solution)/shard_map/all_to_all | solution.py:53
  300.5 1.3 copy-start.5
  414.5 13.5 %copy-start.3 = (f32[256,2]{0,1:T(2,128)S(1)}, f32[256,2]{0,1:T(2,128)}, u32[]{:S(2)}) copy-start(f32[256,2]{0,1:T(2,128)} %param.29) | copy-start | bytes 6148
  421.2 29.0 %all-to-all-start.5 = ((bf16[32,32,128]{2,1,0:T(8,128)(2,1)}), bf16[32,32,128]{2,1,0:T(8,128)(2,1)S(1)}, u32[]{:S(2)}, u32[]{:S(2)}) async-start(bf16[32,32,128]{2,1,0:T(8,128)(2,1)} %bitcast.153), calls=%async_computation.5 | async-start | bytes 524288 | tf_op jit(solution)/shard_map/all_to_all | solution.py:212
Sparse Core Ops, SparseCore 0:
  9.5 79.1 all-gather.1
